TPU v7x, 32 devices: a whole 2x2x4 slice. The times are simulated.
32 devices in a mesh: sp: 16 (over z, y, core), tp: 2 (over x).
Axes of the slice: x: 2, y: 2, z: 4, core: 2. Of those that a mesh axis runs over, the one named last changes fastest.
Arguments:
- queries: bfloat16 [8192, 1024], P('sp', 'tp'), may hold values from -160 to 160
- keys: bfloat16 [8192, 256], P('sp', 'tp'), may hold values from -5 to 5
- values: bfloat16 [8192, 256], P('sp', 'tp'), may hold values from -6 to 6
- doc_ids: int32 [8192], P('sp'), may hold values from 0 to 7, never falling along the last dimension, each value on 1 to 2048 neighbouring positions
- sink_logit: float32 [16], P('tp'), may hold values from 1 to 6
- w_out: bfloat16 [1024, 2048], P('tp'), may hold values from -0.1875 to 0.1875
- residual: bfloat16 [8192, 2048], P(('sp', 'tp')), may hold values from -6 to 6
- ffn_gain: float32 [2048], replicated, may hold values from 0.1 to 1.9
- expert_ids: int32 [8192, 8], P(('sp', 'tp')), may hold values from 0 to 15, all different within a row; in each aligned block of 128 rows (0 to 127, 128 to 255, ...) at most 96 rows name the same one
- expert_weight: float32 [8192, 8], P(('sp', 'tp')), may hold values from 0.2 to 2
- exp_gate: bfloat16 [16, 2048, 512], P('sp'), may hold values from -0.125 to 0.125
- exp_up: bfloat16 [16, 2048, 512], P('sp'), may hold values from -0.125 to 0.125
- exp_down: bfloat16 [16, 512, 2048], P('sp'), may hold values from -0.25 to 0.25
- shared_gate: bfloat16 [2048, 512], P(None, 'tp'), may hold values from -0.125 to 0.125
- shared_up: bfloat16 [2048, 512], P(None, 'tp'), may hold values from -0.125 to 0.125
- shared_down: bfloat16 [512, 2048], P('tp'), may hold values from -0.25 to 0.25
Outputs:
- output: bfloat16 [8192, 2048], P(('sp', 'tp'))
Inputs may be any that keep to these rules, and one draw needn't show every extreme that they name: `doc_ids`: never falling along the sequence; every document holds at most 2048 positions, and one holds exactly that many. `expert_ids`: each row names 8 different experts. In each aligned block of 128 rows no expert is named by more than 96 rows, and in some blocks one expert is named by exactly 96 rows.
All inputs are finite; a program needn't handle non-finite values.
Results may differ from a plain program's by a relative error of at most 0.018.
Values may be sent and summed in bfloat16 or wider, within the bound.
A program may use at most 128 MiB of HBM per device.

v0:
```python
import jax
import jax.numpy as jnp
from jax import lax
from jax.sharding import PartitionSpec as P

HD = 64
WINDOW = 128
norm_eps = 1e-06


def extended(cells, sides, width):
    for axis, dim in sides:
        count = lax.axis_size(axis)
        ends = count - 1
        head = lax.slice_in_dim(cells, 0, width, axis=dim)
        tail = lax.slice_in_dim(cells, cells.shape[dim] - width, cells.shape[dim], axis=dim)
        cells = jnp.concatenate(
            [
                lax.ppermute(tail, axis, [(i, (i + 1) % count) for i in range(ends)]),
                cells,
                lax.ppermute(head, axis, [((i + 1) % count, i) for i in range(ends)]),
            ],
            axis=dim,
        )
    return cells


def band_blocks(padded, width):
    span_count = padded.shape[0] // width - 2
    shaped = padded.reshape((span_count + 2, width) + padded.shape[1:])
    return jnp.concatenate(
        [
            shaped[0:span_count:2],
            shaped[1 : span_count + 1 : 2],
            shaped[2 : span_count + 2 : 2],
            shaped[3 : span_count + 3 : 2],
        ],
        axis=1,
    )


def attend(queries, ext_keys, ext_values, ext_marks, own_marks, sink_logit):
    tok_count = queries.shape[0]
    head_count = sink_logit.shape[0]
    key_heads = ext_keys.shape[1] // HD
    group_size = head_count // key_heads
    query_span = 2 * WINDOW
    block_count = tok_count // query_span
    query_blocks = queries.reshape(block_count, query_span, key_heads, group_size, HD)
    key_blocks = band_blocks(ext_keys, WINDOW).reshape(block_count, 4 * WINDOW, key_heads, HD)
    value_blocks = band_blocks(ext_values, WINDOW).reshape(block_count, 4 * WINDOW, key_heads, HD)
    mark_blocks = band_blocks(ext_marks, WINDOW)
    query_marks = own_marks.reshape(block_count, query_span)
    scores = jnp.einsum(
        "nqkgd,nmkd->nkgqm", query_blocks, key_blocks, preferred_element_type=jnp.float32
    ) * HD ** (-0.5)
    offset = (
        jnp.arange(query_span, dtype=jnp.int32)[:, None]
        - jnp.arange(4 * WINDOW, dtype=jnp.int32)[None, :]
        + WINDOW
    )
    allowed = (jnp.abs(offset) <= WINDOW)[None] & (
        mark_blocks[:, None, :] == query_marks[:, :, None]
    )
    scores = jnp.where(allowed[:, None, None], scores, -jnp.inf)
    sink_term = sink_logit.reshape(key_heads, group_size)[None, :, :, None, None]
    row_max = jnp.maximum(jnp.max(scores, axis=-1, keepdims=True), sink_term)
    exp_scores = jnp.exp(scores - row_max)
    attn_probs = (
        exp_scores / (jnp.sum(exp_scores, axis=-1, keepdims=True) + jnp.exp(sink_term - row_max))
    ).astype(jnp.bfloat16)
    result = jnp.einsum(
        "nkgqm,nmkd->nqkgd", attn_probs, value_blocks, preferred_element_type=jnp.float32
    )
    return result.astype(jnp.bfloat16).reshape(tok_count, head_count * HD)


def slot_index(routing, half_rows, slot_cap, expert_count):
    blocks = routing.shape[0] // half_rows
    flat_ids = routing.reshape(blocks, half_rows * routing.shape[1])
    onehot = (
        flat_ids[:, :, None] == jnp.arange(expert_count, dtype=jnp.int32)[None, None, :]
    ).astype(jnp.int32)
    slot_rank = jnp.sum(jnp.cumsum(onehot, axis=1) * onehot, axis=-1) - 1
    slot_place = (
        flat_ids * (blocks * slot_cap)
        + jnp.arange(blocks, dtype=jnp.int32)[:, None] * slot_cap
        + slot_rank
    )
    return slot_place.reshape(-1)


def pack_rows(normed, slot_place, expert_count, per_expert):
    assign_count = slot_place.shape[0]
    top_count = assign_count // normed.shape[0]
    source = (
        jnp.full((expert_count * per_expert,), normed.shape[0], jnp.int32)
        .at[slot_place]
        .set(jnp.arange(assign_count, dtype=jnp.int32) // top_count)
    )
    packed = jnp.take(normed, source, axis=0, mode="fill", fill_value=0)
    return packed.reshape(expert_count, per_expert, normed.shape[1])


def run_expert(arrived, gate_w, up_w, down_w):
    flat_rows = arrived.reshape(-1, arrived.shape[-1])
    hidden = (
        jax.nn.silu(jnp.dot(flat_rows, gate_w, preferred_element_type=jnp.float32))
        * jnp.dot(flat_rows, up_w, preferred_element_type=jnp.float32)
    ).astype(jnp.bfloat16)
    return (
        jnp.dot(hidden, down_w, preferred_element_type=jnp.float32)
        .astype(jnp.bfloat16)
        .reshape(arrived.shape)
    )


def combine_rows(returned, slot_place, weights):
    picked = returned.reshape(-1, returned.shape[-1])[slot_place].reshape(
        weights.shape + (returned.shape[-1],)
    )
    return jnp.sum(weights[:, :, None] * picked.astype(jnp.float32), axis=1)


def shards(
    queries,
    keys,
    values,
    doc_ids,
    sink_logit,
    w_out,
    residual,
    ffn_gain,
    expert_ids,
    expert_weight,
    exp_gate,
    exp_up,
    exp_down,
    shared_gate,
    shared_up,
    shared_down,
):
    marks = (doc_ids + 1).astype(jnp.bfloat16)
    ext_keys, ext_values, ext_marks = (
        extended(keys, (("sp", 0),), WINDOW),
        extended(values, (("sp", 0),), WINDOW),
        extended(marks, (("sp", 0),), WINDOW),
    )
    attended = attend(queries, ext_keys, ext_values, ext_marks, marks, sink_logit)
    row_count = residual.shape[0]
    mixed = lax.psum_scatter(
        jnp.dot(attended, w_out, preferred_element_type=jnp.float32).astype(jnp.bfloat16),
        "tp",
        scatter_dimension=0,
        tiled=True,
    ).astype(jnp.float32)
    resid = (residual.astype(jnp.float32) + mixed).astype(jnp.bfloat16)
    resid_f = resid.astype(jnp.float32)
    normed = (
        resid_f
        * lax.rsqrt(jnp.mean(resid_f * resid_f, axis=-1, keepdims=True) + norm_eps)
        * ffn_gain
    ).astype(jnp.bfloat16)
    shard_rows = lax.all_gather(normed, "tp", axis=0, tiled=True)
    hidden = (
        jax.nn.silu(jnp.dot(shard_rows, shared_gate, preferred_element_type=jnp.float32))
        * jnp.dot(shard_rows, shared_up, preferred_element_type=jnp.float32)
    ).astype(jnp.bfloat16)
    partial_out = jnp.dot(hidden, shared_down, preferred_element_type=jnp.float32)
    shared_terms = lax.optimization_barrier(partial_out.astype(jnp.bfloat16)).astype(jnp.float32)
    shared_out = lax.psum_scatter(
        shared_terms.astype(jnp.bfloat16), "tp", scatter_dimension=0, tiled=True
    ).astype(jnp.float32)
    expert_count = lax.axis_size("sp") * exp_gate.shape[0]
    top_count = expert_ids.shape[1]
    half_rows = row_count // 2
    slot_cap = min(half_rows, max(2, 3 * half_rows * top_count // (2 * expert_count)))
    halves_out = []
    for half_index in range(2):
        first_row = half_index * half_rows
        part_ids = expert_ids[first_row : first_row + half_rows]
        part_rows = normed[first_row : first_row + half_rows]
        part_weight = expert_weight[first_row : first_row + half_rows]
        slot_place = slot_index(part_ids, half_rows, slot_cap, expert_count)
        packed = pack_rows(part_rows, slot_place, expert_count, slot_cap)
        returned = lax.all_to_all(
            run_expert(
                lax.all_to_all(packed, "sp", split_axis=0, concat_axis=0, tiled=True),
                exp_gate[0],
                exp_up[0],
                exp_down[0],
            ),
            "sp",
            split_axis=0,
            concat_axis=0,
            tiled=True,
        )
        halves_out.append(combine_rows(returned, slot_place, part_weight))
    routed = jnp.concatenate(halves_out, axis=0)
    return (resid.astype(jnp.float32) + shared_out + routed).astype(jnp.bfloat16)


def solution(mesh):
    placed = (
        P("sp", "tp"),
        P("sp", "tp"),
        P("sp", "tp"),
        P("sp"),
        P("tp"),
        P("tp", None),
        P(("sp", "tp"), None),
        P(),
        P(("sp", "tp"), None),
        P(("sp", "tp"), None),
        P("sp", None, None),
        P("sp", None, None),
        P("sp", None, None),
        P(None, "tp"),
        P(None, "tp"),
        P("tp", None),
    )
    return jax.shard_map(
        shards, mesh=mesh, in_specs=placed, out_specs=P(("sp", "tp"), None), check_vma=False
    )
```

profile of v0, /device:TPU:13, one launch (start us, length us, event | category | flops | bytes accessed | tf_op | source)
XLA Modules:
  0.0 713.2 jit_solution(18196577709892937796)
XLA Ops:
  46.2 5.8 fusion.21
  60.8 4.8 scatter_custom_fusion
  65.7 22.6 %reduce-scatter.3.cloned.1.call-done = bf16[256,2048]{1,0:T(8,128)(2,1)} async-done(((bf16[512,2048]{1,0:T(8,128)(2,1)}), bf16[256,2048]{1,0:T(8,128)(2,1)}) %reduce-scatter.3.cloned.1.call-update) | async-done | bytes 1048592 | tf_op jit(solution)/shard_map/reduce_scatter | solution.py:151
  93.8 7.1 %gather_fusion.2 = bf16[1536,2048]{1,0:T(8,128)(2,1)} fusion(bf16[128,2048]{1,0:T(8,128)(2,1)S(1)} %get-tuple-element.6, s32[2048]{0:T(1024)S(1)} %pad_clamp_fusion.1), kind=kCustom, calls=%fused_computation.clone | custom fusion | bytes 12589056 | tf_op jit(solution)/shard_map/jit(_take)/gather | solution.py:101
  100.9 5.9 broadcast_select_fusion.1
  106.8 6.5 all-to-all-start
  123.1 7.1 gather_fusion.3
  130.2 5.9 broadcast_select_fusion
  136.2 114.5 %all-to-all-done = bf16[16,96,2048]{2,1,0:T(8,128)(2,1)} async-done(((bf16[16,96,2048]{2,1,0:T(8,128)(2,1)}), bf16[16,96,2048]{2,1,0:T(8,128)(2,1)}, u32[]{:S(2)}, u32[]{:S(2)}) %all-to-all-start) | async-done | bytes 6291488 | tf_op jit(solution)/shard_map/all_to_all | solution.py:188
  250.7 4.8 all-to-all-start.2
  255.5 8.6 %fusion.18 = f32[1536,512]{1,0:T(8,128)} fusion(bf16[1536,2048]{1,0:T(8,128)(2,1)} %bitcast.18, bf16[1,2048,512]{2,1,0:T(8,128)(2,1)} %param.28), kind=kOutput, calls=%fused_computation.40 | convolution fusion | flops 3221225472 | bytes 11534336 | tf_op jit(solution)/shard_map/dot_general | solution.py:108
  264.1 11.7 %convolution_convert_fusion.1 = bf16[1536,2048]{1,0:T(8,128)(2,1)} fusion(bf16[1,512,2048]{2,1,0:T(8,128)(2,1)S(1)} %copy-done, bf16[1536,2048]{1,0:T(8,128)(2,1)} %bitcast.18, f32[1536,512]{1,0:T(8,128)} %fusion.18, bf16[1,2048,512]{2,1,0:T(8,128)(2,1)} %param.29), kind=kOutput, calls=%fused_computation.14 | convolution fusion | flops 6450315264 | bytes 19922944 | tf_op jit(solution)/shard_map/dot_general | solution.py:112
  275.8 117.1 %all-to-all-done.2 = bf16[16,96,2048]{2,1,0:T(8,128)(2,1)} async-done(((bf16[16,96,2048]{2,1,0:T(8,128)(2,1)}), bf16[16,96,2048]{2,1,0:T(8,128)(2,1)}, u32[]{:S(2)}, u32[]{:S(2)}) %all-to-all-start.2) | async-done | bytes 6291488 | tf_op jit(solution)/shard_map/all_to_all | solution.py:188
  392.9 5.1 all-to-all-start.1
  398.0 8.6 %fusion.16 = f32[1536,512]{1,0:T(8,128)} fusion(bf16[1536,2048]{1,0:T(8,128)(2,1)} %bitcast.32, bf16[1,2048,512]{2,1,0:T(8,128)(2,1)} %param.28), kind=kOutput, calls=%fused_computation.38 | convolution fusion | flops 3221225472 | bytes 11534336 | tf_op jit(solution)/shard_map/dot_general | solution.py:108
  406.6 11.7 %convolution_convert_fusion = bf16[1536,2048]{1,0:T(8,128)(2,1)} fusion(bf16[1,512,2048]{2,1,0:T(8,128)(2,1)S(1)} %copy-done, bf16[1536,2048]{1,0:T(8,128)(2,1)} %bitcast.32, f32[1536,512]{1,0:T(8,128)} %fusion.16, bf16[1,2048,512]{2,1,0:T(8,128)(2,1)} %param.29), kind=kOutput, calls=%fused_computation.13 | convolution fusion | flops 6450315264 | bytes 19922944 | tf_op jit(solution)/shard_map/dot_general | solution.py:112
  418.3 117.0 %all-to-all-done.1 = bf16[16,96,2048]{2,1,0:T(8,128)(2,1)} async-done(((bf16[16,96,2048]{2,1,0:T(8,128)(2,1)}), bf16[16,96,2048]{2,1,0:T(8,128)(2,1)}, u32[]{:S(2)}, u32[]{:S(2)}) %all-to-all-start.1) | async-done | bytes 6291488 | tf_op jit(solution)/shard_map/all_to_all | solution.py:186
  540.8 34.2 %all-gather.2.cloned.1.call-done = bf16[512,2048]{1,0:T(8,128)(2,1)} async-done(((bf16[256,2048]{1,0:T(8,128)(2,1)}), bf16[512,2048]{1,0:T(8,128)(2,1)}) %all-gather.2.cloned.1.call-update) | async-done | bytes 2097168 | tf_op jit(solution)/shard_map/all_gather | solution.py:164
  577.6 5.8 convolution_convert_fusion.2
  583.7 12.6 %gather_fusion = bf16[1024,2048]{1,0:T(8,128)(2,1)} fusion(bf16[1536,2048]{1,0:T(8,128)(2,1)} %bitcast.23, s32[1024]{0:T(1024)S(1)} %broadcast_clamp_fusion.1), kind=kCustom, calls=%fused_computation.2 | custom fusion | bytes 8392704 | tf_op jit(solution)/shard_map/gather | solution.py:119
  596.3 81.1 %all-to-all-done.3 = bf16[16,96,2048]{2,1,0:T(8,128)(2,1)} async-done(((bf16[16,96,2048]{2,1,0:T(8,128)(2,1)}), bf16[16,96,2048]{2,1,0:T(8,128)(2,1)}, u32[]{:S(2)}, u32[]{:S(2)}) %all-to-all-start.3) | async-done | bytes 6291488 | tf_op jit(solution)/shard_map/all_to_all | solution.py:186
  677.4 12.4 %gather_fusion.1 = bf16[1024,2048]{1,0:T(8,128)(2,1)} fusion(bf16[1536,2048]{1,0:T(8,128)(2,1)} %bitcast.34, s32[1024]{0:T(1024)S(1)} %broadcast_clamp_fusion), kind=kCustom, calls=%fused_computation.3 | custom fusion | bytes 8392704 | tf_op jit(solution)/shard_map/gather | solution.py:119
  689.8 7.6 %fusion.1 = f32[128,2048]{1,0:T(8,128)} fusion(bf16[1024,2048]{1,0:T(8,128)(2,1)} %gather_fusion, f32[128,8]{1,0:T(8,128)S(1)} %copy.45), kind=kLoop, calls=%fused_computation.9 | loop fusion | flops 6029312 | bytes 5246976 | tf_op jit(solution)/shard_map/reduce_sum | solution.py:122
  697.4 5.3 fusion
  (132 shorter events, 75.5 us)
Async XLA Ops:
  6.5 257.5 %copy-start = (bf16[1,512,2048]{2,1,0:T(8,128)(2,1)S(1)}, bf16[1,512,2048]{2,1,0:T(8,128)(2,1)}, u32[]{:S(2)}) copy-start(bf16[1,512,2048]{2,1,0:T(8,128)(2,1)} %param.30) | copy-start | bytes 6291460
  6.5 81.7 %reduce-scatter.3.cloned.1.call-start = ((), (), s32[]{:S(2)}) async-start(), calls=%async_computation.6 | async-start | bytes 3145728 | tf_op jit(solution)/shard_map/reduce_scatter | solution.py:151
  7.4 22.5 %collective-permute-start.2 = (bf16[128]{0:T(256)(128)(2,1)S(1)}, bf16[128]{0:T(256)(128)(2,1)S(1)}, u32[]{:S(2)}, u32[]{:S(2)}) collective-permute-start(bf16[128]{0:T(256)(128)(2,1)S(1)} %get-tuple-element.26), channel_id=1, source_target_pairs={{0,2},{2,4},{4,6},{6,8},{8,10},{10,12},{12,14},{14,16},{16,18},{18... | collective-permute-start | bytes 776 | tf_op jit(solution)/shard_map/ppermute | solution.py:19
  11.1 20.8 %collective-permute-start.3 = (bf16[128]{0:T(256)(128)(2,1)S(1)}, bf16[128]{0:T(256)(128)(2,1)S(1)}, u32[]{:S(2)}, u32[]{:S(2)}) collective-permute-start(bf16[128]{0:T(256)(128)(2,1)S(1)} %get-tuple-element.27), channel_id=1, source_target_pairs={{2,0},{4,2},{6,4},{8,6},{10,8},{12,10},{14,12},{16,14},{18,16},{20... | collective-permute-start | bytes 776 | tf_op jit(solution)/shard_map/ppermute | solution.py:21
  14.4 17.8 %collective-permute-start.4 = (bf16[128,128]{1,0:T(8,128)(2,1)}, bf16[128,128]{1,0:T(8,128)(2,1)}, u32[]{:S(2)}, u32[]{:S(2)}) collective-permute-start(bf16[128,128]{1,0:T(8,128)(2,1)} %get-tuple-element.16), channel_id=1, source_target_pairs={{0,2},{2,4},{4,6},{6,8},{8,10},{10,12},{12,14},{14,16},{16,18},{18... | collective-permute-start | bytes 98312 | tf_op jit(solution)/shard_map/ppermute | solution.py:19
  19.0 13.3 %collective-permute-start.5 = (bf16[128,128]{1,0:T(8,128)(2,1)}, bf16[128,128]{1,0:T(8,128)(2,1)}, u32[]{:S(2)}, u32[]{:S(2)}) collective-permute-start(bf16[128,128]{1,0:T(8,128)(2,1)} %get-tuple-element.17), channel_id=1, source_target_pairs={{2,0},{4,2},{6,4},{8,6},{10,8},{12,10},{14,12},{16,14},{18,16},{20... | collective-permute-start | bytes 98312 | tf_op jit(solution)/shard_map/ppermute | solution.py:21
  22.3 22.5 %collective-permute-start = (bf16[128,128]{1,0:T(8,128)(2,1)}, bf16[128,128]{1,0:T(8,128)(2,1)}, u32[]{:S(2)}, u32[]{:S(2)}) collective-permute-start(bf16[128,128]{1,0:T(8,128)(2,1)} %get-tuple-element.18), channel_id=1, source_target_pairs={{0,2},{2,4},{4,6},{6,8},{8,10},{10,12},{12,14},{14,16},{16,18},{18... | collective-permute-start | bytes 98312 | tf_op jit(solution)/shard_map/ppermute | solution.py:19
  29.9 14.8 %collective-permute-start.1 = (bf16[128,128]{1,0:T(8,128)(2,1)}, bf16[128,128]{1,0:T(8,128)(2,1)}, u32[]{:S(2)}, u32[]{:S(2)}) collective-permute-start(bf16[128,128]{1,0:T(8,128)(2,1)} %get-tuple-element.19), channel_id=1, source_target_pairs={{2,0},{4,2},{6,4},{8,6},{10,8},{12,10},{14,12},{16,14},{18,16},{20... | collective-permute-start | bytes 98312 | tf_op jit(solution)/shard_map/ppermute | solution.py:21
  41.4 3.2 copy-start.1
  41.5 3.2 copy-start.5
  46.2 6.5 copy-start.9
  52.7 2.7 copy-start.7
  55.3 32.9 %copy-start.3 = (bf16[256,2048]{1,0:T(8,128)(2,1)S(1)}, bf16[256,2048]{1,0:T(8,128)(2,1)}, u32[]{:S(2)}) copy-start(bf16[256,2048]{1,0:T(8,128)(2,1)} %param.24) | copy-start | bytes 3145732
  55.3 34.6 %copy-start.6 = (f32[2048]{0:T(1024)S(1)}, f32[2048]{0:T(1024)}, u32[]{:S(2)}) copy-start(f32[2048]{0:T(1024)} %param.25) | copy-start | bytes 24580
  106.8 143.9 %all-to-all-start = ((bf16[16,96,2048]{2,1,0:T(8,128)(2,1)}), bf16[16,96,2048]{2,1,0:T(8,128)(2,1)}, u32[]{:S(2)}, u32[]{:S(2)}) async-start(bf16[16,96,2048]{2,1,0:T(8,128)(2,1)} %bitcast.114), calls=%async_computation.2 | async-start | bytes 12582912 | tf_op jit(solution)/shard_map/all_to_all | solution.py:188
  250.7 142.2 %all-to-all-start.2 = ((bf16[16,96,2048]{2,1,0:T(8,128)(2,1)}), bf16[16,96,2048]{2,1,0:T(8,128)(2,1)}, u32[]{:S(2)}, u32[]{:S(2)}) async-start(bf16[16,96,2048]{2,1,0:T(8,128)(2,1)} %bitcast.115), calls=%async_computation.4 | async-start | bytes 12582912 | tf_op jit(solution)/shard_map/all_to_all | solution.py:188
  392.9 142.4 %all-to-all-start.1 = ((bf16[16,96,2048]{2,1,0:T(8,128)(2,1)}), bf16[16,96,2048]{2,1,0:T(8,128)(2,1)}, u32[]{:S(2)}, u32[]{:S(2)}) async-start(bf16[16,96,2048]{2,1,0:T(8,128)(2,1)} %bitcast.117), calls=%async_computation.3 | async-start | bytes 12582912 | tf_op jit(solution)/shard_map/all_to_all | solution.py:186
  535.2 142.2 %all-to-all-start.3 = ((bf16[16,96,2048]{2,1,0:T(8,128)(2,1)}), bf16[16,96,2048]{2,1,0:T(8,128)(2,1)}, u32[]{:S(2)}, u32[]{:S(2)}) async-start(bf16[16,96,2048]{2,1,0:T(8,128)(2,1)} %bitcast.116), calls=%async_computation.5 | async-start | bytes 12582912 | tf_op jit(solution)/shard_map/all_to_all | solution.py:186
  540.0 35.0 %all-gather.2.cloned.1.call-start = ((), (), s32[]{:S(2)}) async-start(), calls=%async_computation.7 | async-start | bytes 3145728 | tf_op jit(solution)/shard_map/all_gather | solution.py:164
  540.7 162.0 %reduce-scatter.5.cloned.1.call-start = ((), (), s32[]{:S(2)}) async-start(), calls=%async_computation.8 | async-start | bytes 3145728 | tf_op jit(solution)/shard_map/reduce_scatter | solution.py:171
  577.6 5.9 copy-start.8
  689.8 7.6 %copy-start.2 = (bf16[1024,2048]{1,0:T(8,128)(2,1)S(1)}, bf16[1024,2048]{1,0:T(8,128)(2,1)}, u32[]{:S(2)}) copy-start(bf16[1024,2048]{1,0:T(8,128)(2,1)} %gather_fusion.1) | copy-start | bytes 12582916
  697.4 5.3 copy-start.4
Sparse Core Ops, SparseCore 0:
  55.4 32.7 reduce-scatter.2
  542.4 32.5 all-gather.1
  583.5 31.8 reduce-scatter.4
where the time goes:
time: 722 us; the launch traced here: 713 us
  waiting for transfers between devices  487 us (67%)
  local copies, waits for them, and re-layouts  65.4 us (9%)
  matrix products  59.3 us (8%)
  other arithmetic  47.8 us (7%)
  starting transfers between devices  39.7 us (5%)
  between operations  13.8 us (2%)
    all_to_all x2, waiting for transfers between devices, shards(): lax.all_to_all(packed, 'sp', split_axis=0, concat_axis=0, tiled=True)  232 us
    all_to_all x2, waiting for transfers between devices, shards(): lax.all_to_all(run_expert(lax.all_to_all(packed, 'sp', split_axis=0, conc...  198 us
    all_gather x1, waiting for transfers between devices, shards(): shard_rows = lax.all_gather(normed, 'tp', axis=0, tiled=True)  34.2 us
    gather x2, local copies, waits for them, and re-layouts, combine_rows(): returned.reshape(-1, returned.shape[-1])[slot_place]  25.1 us
    dot_general x2, matrix products, run_expert(): jnp.dot(hidden, down_w, preferred_element_type=jnp.float32)  23.4 us
    reduce_scatter x1, waiting for transfers between devices, shards(): lax.psum_scatter(jnp.dot(attended, w_out, preferred_element_type=jnp.floa...  22.6 us
    dot_general x2, matrix products, run_expert(): jnp.dot(flat_rows, gate_w, preferred_element_type=jnp.float32)  17.2 us
  transfers between devices with their start and end apart: 13, of which 6 were waited for; matrix products, arithmetic and copies ran while one was open for 19% of the time, Pallas kernels for 0%

commit v1 on v0

--- a/solution.py
+++ b/solution.py
@@ -161,7 +161,9 @@
         * lax.rsqrt(jnp.mean(resid_f * resid_f, axis=-1, keepdims=True) + norm_eps)
         * ffn_gain
     ).astype(jnp.bfloat16)
-    shard_rows = lax.all_gather(normed, "tp", axis=0, tiled=True)
+    local_part = jnp.stack([normed for _ in range(lax.axis_size("tp"))], 0)
+    arr_now = lax.all_to_all(local_part, "tp", 0, 0)
+    shard_rows = jnp.concatenate(arr_now, 0)
     hidden = (
         jax.nn.silu(jnp.dot(shard_rows, shared_gate, preferred_element_type=jnp.float32))
         * jnp.dot(shard_rows, shared_up, preferred_element_type=jnp.float32)

time: 722 us -> 739 us (1.024)
  waiting for transfers between devices: 487 us -> 498 us
    all_to_all x2, waiting for transfers between devices: 198 us -> 233 us  [shards(): lax.all_to_all(run_expert(lax.all_to_all(packed, 'sp', split_axis=0, conc...]
    all_gather x1 -> x0, waiting for transfers between devices: 34.2 us -> none  [shards(): shard_rows = lax.all_gather(normed, 'tp', axis=0, tiled=True)]
    all_to_all x0 -> x1, waiting for transfers between devices: none -> 11.1 us  [shards(): arr_now = lax.all_to_all(local_part, 'tp', 0, 0)]
  transfers between devices with their start and end apart: 13 -> 13, of which waited for: 6 -> 6; matrix products, arithmetic and copies ran while one was open for 19% -> 21% of each run, Pallas kernels for 0% -> 0%
where the time goes in v1:
time: 739 us; the launch traced here: 730 us
  waiting for transfers between devices  498 us (67%)
  local copies, waits for them, and re-layouts  64.3 us (9%)
  matrix products  59.4 us (8%)
  other arithmetic  48.4 us (7%)
  starting transfers between devices  45.3 us (6%)
  between operations  14.2 us (2%)
    all_to_all x2, waiting for transfers between devices, shards(): lax.all_to_all(run_expert(lax.all_to_all(packed, 'sp', split_axis=0, conc...  233 us
    all_to_all x2, waiting for transfers between devices, shards(): lax.all_to_all(packed, 'sp', split_axis=0, concat_axis=0, tiled=True)  232 us
    gather x2, local copies, waits for them, and re-layouts, combine_rows(): returned.reshape(-1, returned.shape[-1])[slot_place]  25.1 us
    dot_general x2, matrix products, run_expert(): jnp.dot(hidden, down_w, preferred_element_type=jnp.float32)  23.5 us
    reduce_scatter x1, waiting for transfers between devices, shards(): lax.psum_scatter(jnp.dot(attended, w_out, preferred_element_type=jnp.floa...  22.6 us
    dot_general x2, matrix products, run_expert(): jnp.dot(flat_rows, gate_w, preferred_element_type=jnp.float32)  17.2 us
  transfers between devices with their start and end apart: 13, of which 6 were waited for; matrix products, arithmetic and copies ran while one was open for 21% of the time, Pallas kernels for 0%

profile of v1, /device:TPU:13, one launch (start us, length us, event | category | flops | bytes accessed | tf_op | source)
XLA Modules:
  0.0 729.7 jit_solution(13917517417858374231)
XLA Ops:
  46.2 5.8 fusion.21
  60.8 4.8 scatter_custom_fusion
  65.7 22.6 %reduce-scatter.3.cloned.1.call-done = bf16[256,2048]{1,0:T(8,128)(2,1)} async-done(((bf16[512,2048]{1,0:T(8,128)(2,1)}), bf16[256,2048]{1,0:T(8,128)(2,1)}) %reduce-scatter.3.cloned.1.call-update) | async-done | bytes 1048592 | tf_op jit(solution)/shard_map/reduce_scatter | solution.py:151
  93.2 4.8 all-to-all-start
  98.0 7.1 gather_fusion.2
  105.1 5.9 broadcast_select_fusion.1
  111.0 11.1 %all-to-all-done = bf16[2,256,2048]{2,1,0:T(8,128)(2,1)} async-done(((bf16[2,256,2048]{2,1,0:T(8,128)(2,1)}), bf16[2,256,2048]{2,1,0:T(8,128)(2,1)}, u32[]{:S(2)}, u32[]{:S(2)}) %all-to-all-start) | async-done | bytes 2097184 | tf_op jit(solution)/shard_map/all_to_all | solution.py:165
  122.1 7.3 %all-to-all-start.1 = ((bf16[16,96,2048]{2,1,0:T(8,128)(2,1)}), bf16[16,96,2048]{2,1,0:T(8,128)(2,1)}, u32[]{:S(2)}, u32[]{:S(2)}) async-start(bf16[16,96,2048]{2,1,0:T(8,128)(2,1)} %bitcast.116), calls=%async_computation.3 | async-start | bytes 12582912 | tf_op jit(solution)/shard_map/all_to_all | solution.py:190
  139.3 7.1 gather_fusion.3
  146.4 5.9 broadcast_select_fusion
  152.3 114.5 %all-to-all-done.1 = bf16[16,96,2048]{2,1,0:T(8,128)(2,1)} async-done(((bf16[16,96,2048]{2,1,0:T(8,128)(2,1)}), bf16[16,96,2048]{2,1,0:T(8,128)(2,1)}, u32[]{:S(2)}, u32[]{:S(2)}) %all-to-all-start.1) | async-done | bytes 6291488 | tf_op jit(solution)/shard_map/all_to_all | solution.py:190
  271.7 8.6 %fusion.18 = f32[1536,512]{1,0:T(8,128)} fusion(bf16[1536,2048]{1,0:T(8,128)(2,1)} %bitcast.20, bf16[1,2048,512]{2,1,0:T(8,128)(2,1)} %param.28), kind=kOutput, calls=%fused_computation.41 | convolution fusion | flops 3221225472 | bytes 11534336 | tf_op jit(solution)/shard_map/dot_general | solution.py:108
  280.3 11.8 %convolution_convert_fusion.1 = bf16[1536,2048]{1,0:T(8,128)(2,1)} fusion(bf16[1,512,2048]{2,1,0:T(8,128)(2,1)S(1)} %copy-done, bf16[1536,2048]{1,0:T(8,128)(2,1)} %bitcast.20, f32[1536,512]{1,0:T(8,128)} %fusion.18, bf16[1,2048,512]{2,1,0:T(8,128)(2,1)} %param.29), kind=kOutput, calls=%fused_computation.14 | convolution fusion | flops 6450315264 | bytes 19922944 | tf_op jit(solution)/shard_map/dot_general | solution.py:112
  292.0 117.0 %all-to-all-done.3 = bf16[16,96,2048]{2,1,0:T(8,128)(2,1)} async-done(((bf16[16,96,2048]{2,1,0:T(8,128)(2,1)}), bf16[16,96,2048]{2,1,0:T(8,128)(2,1)}, u32[]{:S(2)}, u32[]{:S(2)}) %all-to-all-start.3) | async-done | bytes 6291488 | tf_op jit(solution)/shard_map/all_to_all | solution.py:190
  409.1 5.1 all-to-all-start.2
  414.2 8.6 %fusion.16 = f32[1536,512]{1,0:T(8,128)} fusion(bf16[1536,2048]{1,0:T(8,128)(2,1)} %bitcast.34, bf16[1,2048,512]{2,1,0:T(8,128)(2,1)} %param.28), kind=kOutput, calls=%fused_computation.39 | convolution fusion | flops 3221225472 | bytes 11534336 | tf_op jit(solution)/shard_map/dot_general | solution.py:108
  422.8 11.7 %convolution_convert_fusion = bf16[1536,2048]{1,0:T(8,128)(2,1)} fusion(bf16[1,512,2048]{2,1,0:T(8,128)(2,1)S(1)} %copy-done, bf16[1536,2048]{1,0:T(8,128)(2,1)} %bitcast.34, f32[1536,512]{1,0:T(8,128)} %fusion.16, bf16[1,2048,512]{2,1,0:T(8,128)(2,1)} %param.29), kind=kOutput, calls=%fused_computation.13 | convolution fusion | flops 6450315264 | bytes 19922944 | tf_op jit(solution)/shard_map/dot_general | solution.py:112
  434.5 116.9 %all-to-all-done.2 = bf16[16,96,2048]{2,1,0:T(8,128)(2,1)} async-done(((bf16[16,96,2048]{2,1,0:T(8,128)(2,1)}), bf16[16,96,2048]{2,1,0:T(8,128)(2,1)}, u32[]{:S(2)}, u32[]{:S(2)}) %all-to-all-start.2) | async-done | bytes 6291488 | tf_op jit(solution)/shard_map/all_to_all | solution.py:188
  558.8 5.8 convolution_convert_fusion.2
  564.9 12.6 %gather_fusion = bf16[1024,2048]{1,0:T(8,128)(2,1)} fusion(bf16[1536,2048]{1,0:T(8,128)(2,1)} %bitcast.25, s32[1024]{0:T(1024)S(1)} %broadcast_clamp_fusion.1), kind=kCustom, calls=%fused_computation.2 | custom fusion | bytes 8392704 | tf_op jit(solution)/shard_map/gather | solution.py:119
  577.6 116.0 %all-to-all-done.4 = bf16[16,96,2048]{2,1,0:T(8,128)(2,1)} async-done(((bf16[16,96,2048]{2,1,0:T(8,128)(2,1)}), bf16[16,96,2048]{2,1,0:T(8,128)(2,1)}, u32[]{:S(2)}, u32[]{:S(2)}) %all-to-all-start.4) | async-done | bytes 6291488 | tf_op jit(solution)/shard_map/all_to_all | solution.py:188
  693.6 12.4 %gather_fusion.1 = bf16[1024,2048]{1,0:T(8,128)(2,1)} fusion(bf16[1536,2048]{1,0:T(8,128)(2,1)} %bitcast.36, s32[1024]{0:T(1024)S(1)} %broadcast_clamp_fusion), kind=kCustom, calls=%fused_computation.3 | custom fusion | bytes 8392704 | tf_op jit(solution)/shard_map/gather | solution.py:119
  706.0 7.6 %fusion.1 = f32[128,2048]{1,0:T(8,128)} fusion(bf16[1024,2048]{1,0:T(8,128)(2,1)} %gather_fusion, f32[128,8]{1,0:T(8,128)S(1)} %copy.45), kind=kLoop, calls=%fused_computation.9 | loop fusion | flops 6029312 | bytes 5246976 | tf_op jit(solution)/shard_map/reduce_sum | solution.py:122
  713.6 5.3 fusion
  (132 shorter events, 78.9 us)
Async XLA Ops:
  6.5 273.7 %copy-start = (bf16[1,512,2048]{2,1,0:T(8,128)(2,1)S(1)}, bf16[1,512,2048]{2,1,0:T(8,128)(2,1)}, u32[]{:S(2)}) copy-start(bf16[1,512,2048]{2,1,0:T(8,128)(2,1)} %param.30) | copy-start | bytes 6291460
  6.5 81.7 %reduce-scatter.3.cloned.1.call-start = ((), (), s32[]{:S(2)}) async-start(), calls=%async_computation.7 | async-start | bytes 3145728 | tf_op jit(solution)/shard_map/reduce_scatter | solution.py:151
  7.4 22.5 %collective-permute-start.2 = (bf16[128]{0:T(256)(128)(2,1)S(1)}, bf16[128]{0:T(256)(128)(2,1)S(1)}, u32[]{:S(2)}, u32[]{:S(2)}) collective-permute-start(bf16[128]{0:T(256)(128)(2,1)S(1)} %get-tuple-element.26), channel_id=1, source_target_pairs={{0,2},{2,4},{4,6},{6,8},{8,10},{10,12},{12,14},{14,16},{16,18},{18... | collective-permute-start | bytes 776 | tf_op jit(solution)/shard_map/ppermute | solution.py:19
  11.1 20.8 %collective-permute-start.3 = (bf16[128]{0:T(256)(128)(2,1)S(1)}, bf16[128]{0:T(256)(128)(2,1)S(1)}, u32[]{:S(2)}, u32[]{:S(2)}) collective-permute-start(bf16[128]{0:T(256)(128)(2,1)S(1)} %get-tuple-element.27), channel_id=1, source_target_pairs={{2,0},{4,2},{6,4},{8,6},{10,8},{12,10},{14,12},{16,14},{18,16},{20... | collective-permute-start | bytes 776 | tf_op jit(solution)/shard_map/ppermute | solution.py:21
  14.4 17.8 %collective-permute-start.4 = (bf16[128,128]{1,0:T(8,128)(2,1)}, bf16[128,128]{1,0:T(8,128)(2,1)}, u32[]{:S(2)}, u32[]{:S(2)}) collective-permute-start(bf16[128,128]{1,0:T(8,128)(2,1)} %get-tuple-element.16), channel_id=1, source_target_pairs={{0,2},{2,4},{4,6},{6,8},{8,10},{10,12},{12,14},{14,16},{16,18},{18... | collective-permute-start | bytes 98312 | tf_op jit(solution)/shard_map/ppermute | solution.py:19
  19.0 13.3 %collective-permute-start.5 = (bf16[128,128]{1,0:T(8,128)(2,1)}, bf16[128,128]{1,0:T(8,128)(2,1)}, u32[]{:S(2)}, u32[]{:S(2)}) collective-permute-start(bf16[128,128]{1,0:T(8,128)(2,1)} %get-tuple-element.17), channel_id=1, source_target_pairs={{2,0},{4,2},{6,4},{8,6},{10,8},{12,10},{14,12},{16,14},{18,16},{20... | collective-permute-start | bytes 98312 | tf_op jit(solution)/shard_map/ppermute | solution.py:21
  22.3 22.5 %collective-permute-start = (bf16[128,128]{1,0:T(8,128)(2,1)}, bf16[128,128]{1,0:T(8,128)(2,1)}, u32[]{:S(2)}, u32[]{:S(2)}) collective-permute-start(bf16[128,128]{1,0:T(8,128)(2,1)} %get-tuple-element.18), channel_id=1, source_target_pairs={{0,2},{2,4},{4,6},{6,8},{8,10},{10,12},{12,14},{14,16},{16,18},{18... | collective-permute-start | bytes 98312 | tf_op jit(solution)/shard_map/ppermute | solution.py:19
  29.9 14.8 %collective-permute-start.1 = (bf16[128,128]{1,0:T(8,128)(2,1)}, bf16[128,128]{1,0:T(8,128)(2,1)}, u32[]{:S(2)}, u32[]{:S(2)}) collective-permute-start(bf16[128,128]{1,0:T(8,128)(2,1)} %get-tuple-element.19), channel_id=1, source_target_pairs={{2,0},{4,2},{6,4},{8,6},{10,8},{12,10},{14,12},{16,14},{18,16},{20... | collective-permute-start | bytes 98312 | tf_op jit(solution)/shard_map/ppermute | solution.py:21
  41.4 3.2 copy-start.1
  41.5 3.2 copy-start.5
  46.2 6.5 copy-start.9
  52.7 2.7 copy-start.7
  55.3 32.9 %copy-start.3 = (bf16[256,2048]{1,0:T(8,128)(2,1)S(1)}, bf16[256,2048]{1,0:T(8,128)(2,1)}, u32[]{:S(2)}) copy-start(bf16[256,2048]{1,0:T(8,128)(2,1)} %param.24) | copy-start | bytes 3145732
  55.3 34.6 %copy-start.6 = (f32[2048]{0:T(1024)S(1)}, f32[2048]{0:T(1024)}, u32[]{:S(2)}) copy-start(f32[2048]{0:T(1024)} %param.25) | copy-start | bytes 24580
  93.2 29.0 %all-to-all-start = ((bf16[2,256,2048]{2,1,0:T(8,128)(2,1)}), bf16[2,256,2048]{2,1,0:T(8,128)(2,1)}, u32[]{:S(2)}, u32[]{:S(2)}) async-start(bf16[2,256,2048]{2,1,0:T(8,128)(2,1)} %pad_maximum_fusion), calls=%async_computation.1 | async-start | bytes 4194304 | tf_op jit(solution)/shard_map/all_to_all | solution.py:165
  122.1 144.7 %all-to-all-start.1 = ((bf16[16,96,2048]{2,1,0:T(8,128)(2,1)}), bf16[16,96,2048]{2,1,0:T(8,128)(2,1)}, u32[]{:S(2)}, u32[]{:S(2)}) async-start(bf16[16,96,2048]{2,1,0:T(8,128)(2,1)} %bitcast.116), calls=%async_computation.3 | async-start | bytes 12582912 | tf_op jit(solution)/shard_map/all_to_all | solution.py:190
  266.9 142.2 %all-to-all-start.3 = ((bf16[16,96,2048]{2,1,0:T(8,128)(2,1)}), bf16[16,96,2048]{2,1,0:T(8,128)(2,1)}, u32[]{:S(2)}, u32[]{:S(2)}) async-start(bf16[16,96,2048]{2,1,0:T(8,128)(2,1)} %bitcast.117), calls=%async_computation.5 | async-start | bytes 12582912 | tf_op jit(solution)/shard_map/all_to_all | solution.py:190
  409.1 142.4 %all-to-all-start.2 = ((bf16[16,96,2048]{2,1,0:T(8,128)(2,1)}), bf16[16,96,2048]{2,1,0:T(8,128)(2,1)}, u32[]{:S(2)}, u32[]{:S(2)}) async-start(bf16[16,96,2048]{2,1,0:T(8,128)(2,1)} %bitcast.120), calls=%async_computation.4 | async-start | bytes 12582912 | tf_op jit(solution)/shard_map/all_to_all | solution.py:188
  551.4 142.2 %all-to-all-start.4 = ((bf16[16,96,2048]{2,1,0:T(8,128)(2,1)}), bf16[16,96,2048]{2,1,0:T(8,128)(2,1)}, u32[]{:S(2)}, u32[]{:S(2)}) async-start(bf16[16,96,2048]{2,1,0:T(8,128)(2,1)} %bitcast.119), calls=%async_computation.6 | async-start | bytes 12582912 | tf_op jit(solution)/shard_map/all_to_all | solution.py:188
  556.2 162.7 %reduce-scatter.5.cloned.1.call-start = ((), (), s32[]{:S(2)}) async-start(), calls=%async_computation.8 | async-start | bytes 3145728 | tf_op jit(solution)/shard_map/reduce_scatter | solution.py:173
  558.8 5.9 copy-start.8
  706.0 7.6 %copy-start.2 = (bf16[1024,2048]{1,0:T(8,128)(2,1)S(1)}, bf16[1024,2048]{1,0:T(8,128)(2,1)}, u32[]{:S(2)}) copy-start(bf16[1024,2048]{1,0:T(8,128)(2,1)} %gather_fusion.1) | copy-start | bytes 12582916
  713.6 5.3 copy-start.4
Sparse Core Ops, SparseCore 0:
  55.4 32.7 reduce-scatter.2
  564.8 31.4 reduce-scatter.4
